TPU v7x, 32 devices: a whole 2x2x4 slice. The times are simulated.
32 devices in a mesh: grp: 2 (over x), tp: 4 (over z), dp: 4 (over y, core).
Axes of the slice: x: 2, y: 2, z: 4, core: 2. Of those that a mesh axis runs over, the one named last changes fastest.
Arguments:
- tokens: bfloat16 [32, 4096], P(('grp', 'tp'), 'dp'), parts along dimension 0, may hold values from -30 to 30
- norm_gain: float32 [2, 4096], P(None, 'dp'), may hold values from 0.1 to 1.9
- w_query: bfloat16 [2, 4096, 2048], P(None, 'dp', 'tp'), may hold values from -0.09375 to 0.09375
- w_forget: bfloat16 [2, 4096, 2048], P(None, 'dp', 'tp'), may hold values from -0.09375 to 0.09375
- w_value: bfloat16 [2, 4096, 2048], P(None, 'dp', 'tp'), may hold values from -0.09375 to 0.09375
- w_gate: bfloat16 [2, 4096, 2048], P(None, 'dp', 'tp'), may hold values from -0.09375 to 0.09375
- lower_bound: float32 [2, 2048], P(None, 'tp'), may hold values from 0 to 0.9
- head_gain: float32 [2, 128], replicated, may hold values from 0.1 to 1.9
- w_out: bfloat16 [2, 2048, 4096], P(None, 'tp', 'dp'), may hold values from -0.125 to 0.125
- state: float32 [2, 32, 16, 128, 128], P(None, ('grp', 'dp'), 'tp'), parts along dimension 1, may hold values from -4 to 4
Outputs:
- hidden_out: bfloat16 [32, 4096], P(('grp', 'tp'), 'dp'), parts along dimension 0
- new_state: float32 [2, 32, 16, 128, 128], P(None, ('grp', 'dp'), 'tp'), parts along dimension 1
There are 2 independent parts, one for each index of `grp`. A program takes and returns all parts, laid end to end along the dimension named above; an argument that names none is the same for every part. Nothing has to cross between parts.
All inputs are finite; a program needn't handle non-finite values.
Results may differ from a plain program's by a relative error of at most 0.02.
Values may be sent and summed in bfloat16 or wider, within the bound.
No kernel may reach another device: no remote copies, remote signals or barrier semaphores. Data moves between devices by JAX's collectives and lax.ppermute only.
A program may use at most 64 MiB of HBM per device.

v0:
```python
import jax
import jax.numpy as jnp
from jax import lax
from jax.sharding import PartitionSpec as P

D = 4096
HD = 128


def per_device(
    tokens, norm_gain, w_query, w_forget, w_value, w_gate, lower_bound, head_gain, w_out, state
):
    local_seqs = state.shape[1]
    head_count = state.shape[2]
    offset = lax.axis_index("dp") * local_seqs
    hidden = tokens
    updated = []
    for layer in range(2):
        gathered = lax.all_gather(hidden, "tp", axis=0, tiled=True)
        widened = gathered.astype(jnp.float32)
        squares = jnp.sum(widened * widened, axis=1)
        scaled = (widened * norm_gain[layer]).astype(jnp.bfloat16)
        joined = jnp.concatenate(
            [
                jnp.dot(scaled, weight[layer], preferred_element_type=jnp.float32)
                for weight in (w_query, w_forget, w_value, w_gate)
            ],
            axis=1,
        )
        square_total = lax.psum(squares, "dp")
        own_squares = lax.dynamic_slice_in_dim(square_total, offset, local_seqs, 0)
        payload = (joined,)
        summed = (lax.psum(payload[0].astype(jnp.bfloat16), "dp").astype(jnp.float32),)
        shares = tuple(
            (lax.dynamic_slice_in_dim(member, offset, local_seqs, 0) for member in summed)
        )
        own_proj = shares[0]
        width = own_proj.shape[1] // 4
        factor = lax.rsqrt(own_squares / D + 1e-06)[:, None]
        query, forget_pre, value, gate_pre = (
            own_proj[:, index * width : (index + 1) * width] * factor for index in range(4)
        )
        bound = lower_bound[layer]
        forget = bound + (1.0 - bound) * jax.nn.sigmoid(forget_pre)
        keyvec = (1.0 - bound) * jax.nn.sigmoid(-forget_pre)

        def shaped(array):
            return array.reshape(local_seqs, head_count, HD)

        carried = (
            shaped(forget)[..., None] * state[layer]
            + shaped(keyvec)[..., None] * shaped(value)[..., None, :]
        )
        updated.append(carried)
        readout = jnp.einsum("bhkv,bhk->bhv", carried, shaped(query))
        readout = (
            readout
            * lax.rsqrt(jnp.mean(readout * readout, axis=-1, keepdims=True) + 1e-06)
            * head_gain[layer]
        )
        normed = (readout.reshape(local_seqs, head_count * HD) * jax.nn.sigmoid(gate_pre)).astype(
            jnp.bfloat16
        )
        out_weight = w_out[layer]
        mixed = jnp.dot(
            lax.all_gather(normed, "dp", axis=0, tiled=True),
            out_weight,
            preferred_element_type=jnp.float32,
        )
        mixed_sum = lax.psum_scatter(
            mixed.astype(jnp.bfloat16), "tp", scatter_dimension=0, tiled=True
        ).astype(jnp.float32)
        hidden = (hidden.astype(jnp.float32) + mixed_sum).astype(jnp.bfloat16)
    return (hidden, jnp.stack(updated))


def solution(mesh):
    return jax.shard_map(
        per_device,
        mesh=mesh,
        in_specs=(
            P(("grp", "tp"), "dp"),
            P(None, "dp"),
            P(None, "dp", "tp"),
            P(None, "dp", "tp"),
            P(None, "dp", "tp"),
            P(None, "dp", "tp"),
            P(None, "tp"),
            P(),
            P(None, "tp", "dp"),
            P(None, ("grp", "dp"), "tp", None, None),
        ),
        out_specs=(P(("grp", "tp"), "dp"), P(None, ("grp", "dp"), "tp", None, None)),
        check_vma=False,
    )
```

profile of v0, /device:TPU:0, one launch (start us, length us, event | category | flops | bytes accessed | tf_op | source)
XLA Modules:
  0.0 181.9 jit_solution(1064112044140529132)
XLA Ops:
  7.2 0.0 all-reduce.5.cloned.1.call-start
  7.2 0.9 fusion.47
  8.1 15.1 %all-gather = bf16[4,4,1024]{2,1,0:T(4,128)(2,1)S(1)} all-gather(bf16[1,4,1024]{2,1,0:T(4,128)(2,1)} %bitcast.92), channel_id=1, replica_groups=mesh['grp'=2,'tp'=4,'dp'=4] {'tp'}, dimensions={0}, use_global_device_ids=true | all-gather | bytes 40960 | tf_op jit(solution)/shard_map/all_gather | solution.py:19
  23.2 0.1 multiply_convert_fusion.1
  23.3 0.0 copy-start.7
  23.3 1.5 convolution_convert_fusion.6
  24.8 1.5 convolution_convert_fusion.7
  26.3 0.3 convolution_convert_fusion.8
  26.5 1.6 convolution_convert_fusion.9
  28.2 0.7 pad_maximum_fusion.1
  28.8 0.0 all-reduce.5.cloned.1.call-update
  28.8 0.0 all-reduce.7.cloned.1.call-start
  28.9 5.7 %psum.29 = f32[16]{0:T(128)S(1)} all-reduce(f32[16]{0:T(128)S(1)} %get-tuple-element.7), channel_id=1, replica_groups=mesh['grp'=2,'tp'=4,'dp'=4] {'dp'}, use_global_device_ids=true, to_apply=%region_2.0 | all-reduce | flops 16 | bytes 128 | tf_op jit(solution)/shard_map/psum | solution.py:30
  34.6 0.1 add_rsqrt_fusion.3
  34.7 0.6 dynamic-slice
  35.9 25.6 %all-reduce.5.cloned.1.call-done = bf16[16,2048]{1,0:T(8,128)(2,1)} async-done(((bf16[16,2048]{1,0:T(8,128)(2,1)}), bf16[16,2048]{1,0:T(8,128)(2,1)}) %all-reduce.5.cloned.1.call-update) | async-done | bytes 65552 | tf_op jit(solution)/shard_map/psum | solution.py:33
  61.5 0.8 dynamic-slice_convert_fusion.1
  62.3 0.1 multiply_add_fusion.3
  62.4 1.9 %fusion.10 = f32[4,4,1,128]{3,2,1,0:T(1,128)S(1)} fusion(f32[4,4,128,1]{2,3,1,0:T(1,128)S(1)} %bitcast.100, f32[2,4,4,128,128]{4,3,2,1,0:T(8,128)} %param.19, f32[4,4,128]{2,1,0:T(4,128)S(1)} %mul.268, f32[4,4,128]{2,1,0:T(4,128)S(1)} %mul.265, f32[4,4,128]{2,1,0:T(4,128)S(1)} %mul.261), kind=kOutput, calls=%fused_computation.22 | convolution fusion | flops 1310720 | bytes 1089536 | tf_op jit(solution)/shard_map/bhkv,bhk->bhv/dot_general | solution.py:55
  64.4 0.1 multiply_reduce_fusion.3
  64.5 0.1 multiply_bitcast_fusion.1
  64.5 0.1 fusion.45
  64.6 5.2 %all-gather.1 = bf16[4,4,512]{2,1,0:T(4,128)(2,1)S(1)} all-gather(bf16[1,4,512]{2,1,0:T(4,128)(2,1)S(1)} %fusion.45), channel_id=1, replica_groups=mesh['grp'=2,'tp'=4,'dp'=4] {'dp'}, dimensions={0}, use_global_device_ids=true | all-gather | bytes 20480 | tf_op jit(solution)/shard_map/all_gather | solution.py:66
  69.9 1.5 convolution_convert_fusion.1
  71.3 19.0 %all-reduce = bf16[16,1024]{1,0:T(8,128)(2,1)S(1)} all-reduce(bf16[16,1024]{1,0:T(8,128)(2,1)S(1)} %convolution_convert_fusion.1), channel_id=2, replica_groups=mesh['grp'=2,'tp'=4,'dp'=4] {'tp'}, use_global_device_ids=true, to_apply=%region_4.0.clone | all-reduce | flops 16384 | bytes 65536
  90.4 13.1 %all-gather.2 = bf16[4,4,1024]{2,1,0:T(4,128)(2,1)S(1)} all-gather(bf16[1,4,1024]{2,1,0:T(4,128)(2,1)S(1)} %fusion.46), channel_id=1, replica_groups=mesh['grp'=2,'tp'=4,'dp'=4] {'tp'}, dimensions={0}, use_global_device_ids=true | all-gather | bytes 40960 | tf_op jit(solution)/shard_map/all_gather | solution.py:19
  103.5 0.1 multiply_convert_fusion
  103.6 0.2 convolution_convert_fusion.2
  103.9 1.7 convolution_convert_fusion.3
  105.6 0.3 convolution_convert_fusion.4
  105.8 1.5 convolution_convert_fusion.5
  107.3 5.9 %psum.31 = f32[16]{0:T(128)S(1)} all-reduce(f32[16]{0:T(128)S(1)} %get-tuple-element.5), channel_id=1, replica_groups=mesh['grp'=2,'tp'=4,'dp'=4] {'dp'}, use_global_device_ids=true, to_apply=%region_7.0 | all-reduce | flops 16 | bytes 128 | tf_op jit(solution)/shard_map/psum | solution.py:30
  113.1 0.6 pad_maximum_fusion.2
  113.8 0.0 all-reduce.7.cloned.1.call-update
  113.8 0.1 add_rsqrt_fusion.2
  113.9 28.8 %all-reduce.7.cloned.1.call-done = bf16[16,2048]{1,0:T(8,128)(2,1)} async-done(((bf16[16,2048]{1,0:T(8,128)(2,1)}), bf16[16,2048]{1,0:T(8,128)(2,1)}) %all-reduce.7.cloned.1.call-update) | async-done | bytes 65552 | tf_op jit(solution)/shard_map/psum | solution.py:33
  142.7 0.8 dynamic-slice_convert_fusion
  143.5 0.1 multiply_add_fusion.2
  143.7 2.6 %multiply_add_fusion.1 = (f32[1,4,4,128,128]{4,3,2,1,0:T(8,128)S(1)}, f32[1,4,4,128,128]{4,3,2,1,0:T(8,128)S(1)}) fusion(f32[2,4,4,128,128]{4,3,2,1,0:T(8,128)} %param.19, f32[4,4,128]{2,1,0:T(4,128)S(1)} %mul.268, f32[4,4,128]{2,1,0:T(4,128)S(1)} %mul.265, f32[4,4,128]{2,1,0:T(4,128)S(1)} %mul.261, f32[4,4,128]{2,1,0:T(4,128)S(1)} %mul.296, ...), kind=kLoop, calls=%fused_computation.28 | loop fusion | flops 1572864 | bytes 4243456 | tf_op jit(solution)/shard_map/add | solution.py:51
  146.3 0.7 fusion.2
  147.0 0.1 multiply_reduce_fusion.2
  147.1 0.1 multiply_bitcast_fusion
  147.2 0.1 fusion.44
  147.3 5.2 %all-gather.3 = bf16[4,4,512]{2,1,0:T(4,128)(2,1)S(1)} all-gather(bf16[1,4,512]{2,1,0:T(4,128)(2,1)S(1)} %fusion.44), channel_id=1, replica_groups=mesh['grp'=2,'tp'=4,'dp'=4] {'dp'}, dimensions={0}, use_global_device_ids=true | all-gather | bytes 20480 | tf_op jit(solution)/shard_map/all_gather | solution.py:66
  152.5 1.5 convolution_convert_fusion
  154.0 19.0 %all-reduce.1 = bf16[16,1024]{1,0:T(8,128)(2,1)S(1)} all-reduce(bf16[16,1024]{1,0:T(8,128)(2,1)S(1)} %convolution_convert_fusion), channel_id=3, replica_groups=mesh['grp'=2,'tp'=4,'dp'=4] {'tp'}, use_global_device_ids=true, to_apply=%region_9.0.clone | all-reduce | flops 16384 | bytes 65536
  173.0 0.6 add_convert_fusion
  173.6 1.5 pad_maximum_fusion
  (32 shorter events, 0.2 us)
Async XLA Ops:
  7.2 19.1 %copy-start.1 = (bf16[2,1024,512]{2,1,0:T(8,128)(2,1)S(1)}, bf16[2,1024,512]{2,1,0:T(8,128)(2,1)}, u32[]{:S(2)}) copy-start(bf16[2,1024,512]{2,1,0:T(8,128)(2,1)} %param.13) | copy-start | bytes 6291460
  7.2 54.3 %all-reduce.5.cloned.1.call-start = ((), (), s32[]{:S(2)}) async-start(), calls=%async_computation | async-start | bytes 131072 | tf_op jit(solution)/shard_map/psum | solution.py:33
  23.3 5.6 %copy-start.6 = (f32[2,128]{1,0:T(2,128)S(1)}, f32[2,128]{1,0:T(2,128)}, u32[]{:S(2)}) copy-start(f32[2,128]{1,0:T(2,128)} %param.17) | copy-start | bytes 3076
  23.3 5.6 %copy-start.5 = (f32[2,512]{1,0:T(2,128)S(1)}, f32[2,512]{1,0:T(2,128)}, u32[]{:S(2)}) copy-start(f32[2,512]{1,0:T(2,128)} %param.16) | copy-start | bytes 12292
  23.3 11.4 %copy-start.7 = (u32[32]{0:T(128)S(1)}, u32[32]{0:T(128)}, u32[]{:S(2)}) copy-start(u32[32]{0:T(128)} %constant.30) | copy-start | bytes 388
  26.5 63.8 %copy-start.4 = (bf16[4,1024]{1,0:T(4,128)(2,1)S(1)}, bf16[4,1024]{1,0:T(4,128)(2,1)}, u32[]{:S(2)}) copy-start(bf16[4,1024]{1,0:T(4,128)(2,1)} %param.10) | copy-start | bytes 24580
  26.5 77.1 %copy-start = (bf16[2,1024,512]{2,1,0:T(8,128)(2,1)S(1)}, bf16[2,1024,512]{2,1,0:T(8,128)(2,1)}, u32[]{:S(2)}) copy-start(bf16[2,1024,512]{2,1,0:T(8,128)(2,1)} %param.15) | copy-start | bytes 6291460
  28.8 113.9 %all-reduce.7.cloned.1.call-start = ((), (), s32[]{:S(2)}) async-start(), calls=%async_computation.1 | async-start | bytes 131072 | tf_op jit(solution)/shard_map/psum | solution.py:33
  103.5 2.1 %copy-start.2 = (bf16[2,1024,512]{2,1,0:T(8,128)(2,1)S(1)}, bf16[2,1024,512]{2,1,0:T(8,128)(2,1)}, u32[]{:S(2)}) copy-start(bf16[2,1024,512]{2,1,0:T(8,128)(2,1)} %param.13) | copy-start | bytes 6291460
  143.7 2.6 %copy-start.3 = (f32[2,4,4,128,128]{4,3,2,1,0:T(8,128)S(1)}, f32[2,4,4,128,128]{4,3,2,1,0:T(8,128)}, u32[]{:S(2)}) copy-start(f32[2,4,4,128,128]{4,3,2,1,0:T(8,128)} %param.19) | copy-start | bytes 6291460
Sparse Core Ops, SparseCore 0:
  28.9 32.5 all-reduce.4
  113.9 28.7 all-reduce.6
where the time goes:
time: 182 us
  blocking collectives  88.1 us (48%)
  waiting for transfers between devices  54.5 us (30%)
  between operations  14.9 us (8%)
  matrix products  14.1 us (8%)
  other arithmetic  8.64 us (5%)
    psum x2, waiting for transfers between devices, per_device(): lax.psum(payload[0].astype(jnp.bfloat16), 'dp').astype(jnp.float32)  54.4 us
    unnamed x2, blocking collectives  38 us
    all_gather x2, blocking collectives, per_device(): gathered = lax.all_gather(hidden, 'tp', axis=0, tiled=True)  28.2 us
    psum x2, blocking collectives, per_device(): square_total = lax.psum(squares, 'dp')  11.5 us
    all_gather x2, blocking collectives, per_device(): lax.all_gather(normed, 'dp', axis=0, tiled=True)  10.4 us
    dot_general x8, matrix products, per_device(): jnp.dot(scaled, weight[layer], preferred_element_type=jnp.float32)  8.47 us
  transfers between devices with their start and end apart: 2, of which 2 were waited for; matrix products, arithmetic and copies ran while one was open for 0% of the time, Pallas kernels for 0%

commit v1 on v0

--- a/solution.py
+++ b/solution.py
@@ -27,7 +27,7 @@
             ],
             axis=1,
         )
-        square_total = lax.psum(squares, "dp")
+        square_total = jnp.sum(lax.all_gather(squares, "dp"), axis=0)
         own_squares = lax.dynamic_slice_in_dim(square_total, offset, local_seqs, 0)
         payload = (joined,)
         summed = (lax.psum(payload[0].astype(jnp.bfloat16), "dp").astype(jnp.float32),)

time: 182 us -> 183 us (level)
    psum x2 -> x0, blocking collectives: 11.5 us -> none  [per_device(): square_total = lax.psum(squares, 'dp')]
    unnamed x2 -> x4, blocking collectives: 38 us -> 49.4 us
  transfers between devices with their start and end apart: 2 -> 2, of which waited for: 2 -> 2; matrix products, arithmetic and copies ran while one was open for 0% -> 1% of each run, Pallas kernels for 0% -> 0%
where the time goes in v1:
time: 183 us; the launch traced here: 182 us
  blocking collectives  88 us (48%)
  waiting for transfers between devices  52.9 us (29%)
  between operations  15.5 us (8%)
  matrix products  14.1 us (8%)
  other arithmetic  8.73 us (5%)
  local copies, waits for them, and re-layouts  2.88 us (2%)
    psum x2, waiting for transfers between devices, per_device(): lax.psum(payload[0].astype(jnp.bfloat16), 'dp').astype(jnp.float32)  52.9 us
    unnamed x4, blocking collectives  49.4 us
    all_gather x2, blocking collectives, per_device(): gathered = lax.all_gather(hidden, 'tp', axis=0, tiled=True)  28.2 us
    all_gather x2, blocking collectives, per_device(): lax.all_gather(normed, 'dp', axis=0, tiled=True)  10.4 us
    dot_general x8, matrix products, per_device(): jnp.dot(scaled, weight[layer], preferred_element_type=jnp.float32)  8.48 us
  transfers between devices with their start and end apart: 2, of which 2 were waited for; matrix products, arithmetic and copies ran while one was open for 1% of the time, Pallas kernels for 0%

profile of v1, /device:TPU:0, one launch (start us, length us, event | category | flops | bytes accessed | tf_op | source)
XLA Modules:
  0.0 182.2 jit_solution(7922369420570722631)
XLA Ops:
  7.2 0.9 fusion.47
  8.1 15.1 %all-gather.2 = bf16[4,4,1024]{2,1,0:T(4,128)(2,1)S(1)} all-gather(bf16[1,4,1024]{2,1,0:T(4,128)(2,1)} %bitcast.93), channel_id=1, replica_groups=mesh['grp'=2,'tp'=4,'dp'=4] {'tp'}, dimensions={0}, use_global_device_ids=true | all-gather | bytes 40960 | tf_op jit(solution)/shard_map/all_gather | solution.py:19
  23.2 0.1 multiply_convert_fusion.1
  23.3 1.5 convolution_convert_fusion.6
  24.8 1.5 convolution_convert_fusion.7
  26.3 0.2 convolution_convert_fusion.8
  26.5 1.6 convolution_convert_fusion.9
  28.2 0.7 pad_maximum_fusion.1
  29.0 0.6 dynamic-slice
  30.2 0.2 dynamic-update-slice
  30.5 5.6 %all-reduce = f32[64]{0:T(128)S(1)} all-reduce(f32[64]{0:T(128)S(1)} %dynamic-update-slice), channel_id=2, replica_groups=mesh['grp'=2,'tp'=4,'dp'=4] {'dp'}, use_global_device_ids=true, to_apply=%add | all-reduce | flops 64 | bytes 512
  36.1 0.1 reshape.52
  36.2 0.1 add_rsqrt_fusion.3
  36.3 0.6 dynamic-slice.2
  37.5 24.0 %all-reduce.7.cloned.1.call-done = bf16[16,2048]{1,0:T(8,128)(2,1)} async-done(((bf16[16,2048]{1,0:T(8,128)(2,1)}), bf16[16,2048]{1,0:T(8,128)(2,1)}) %all-reduce.7.cloned.1.call-update) | async-done | bytes 65552 | tf_op jit(solution)/shard_map/psum | solution.py:33
  61.5 0.8 dynamic-slice_convert_fusion.1
  62.3 0.1 multiply_add_fusion.3
  62.4 1.9 %fusion.10 = f32[4,4,1,128]{3,2,1,0:T(1,128)S(1)} fusion(f32[4,4,128,1]{2,3,1,0:T(1,128)S(1)} %bitcast.101, f32[2,4,4,128,128]{4,3,2,1,0:T(8,128)} %param.19, f32[4,4,128]{2,1,0:T(4,128)S(1)} %mul.268, f32[4,4,128]{2,1,0:T(4,128)S(1)} %mul.265, f32[4,4,128]{2,1,0:T(4,128)S(1)} %mul.261), kind=kOutput, calls=%fused_computation.22 | convolution fusion | flops 1310720 | bytes 1089536 | tf_op jit(solution)/shard_map/bhkv,bhk->bhv/dot_general | solution.py:55
  64.4 0.1 multiply_reduce_fusion.3
  64.5 0.1 multiply_bitcast_fusion.1
  64.6 0.1 fusion.45
  64.7 5.2 %all-gather.3 = bf16[4,4,512]{2,1,0:T(4,128)(2,1)S(1)} all-gather(bf16[1,4,512]{2,1,0:T(4,128)(2,1)S(1)} %fusion.45), channel_id=1, replica_groups=mesh['grp'=2,'tp'=4,'dp'=4] {'dp'}, dimensions={0}, use_global_device_ids=true | all-gather | bytes 20480 | tf_op jit(solution)/shard_map/all_gather | solution.py:66
  69.9 1.5 convolution_convert_fusion.1
  71.4 19.0 %all-reduce.2 = bf16[16,1024]{1,0:T(8,128)(2,1)S(1)} all-reduce(bf16[16,1024]{1,0:T(8,128)(2,1)S(1)} %convolution_convert_fusion.1), channel_id=4, replica_groups=mesh['grp'=2,'tp'=4,'dp'=4] {'tp'}, use_global_device_ids=true, to_apply=%region_4.0.clone | all-reduce | flops 16384 | bytes 65536
  90.4 13.1 %all-gather.4 = bf16[4,4,1024]{2,1,0:T(4,128)(2,1)S(1)} all-gather(bf16[1,4,1024]{2,1,0:T(4,128)(2,1)S(1)} %fusion.46), channel_id=1, replica_groups=mesh['grp'=2,'tp'=4,'dp'=4] {'tp'}, dimensions={0}, use_global_device_ids=true | all-gather | bytes 40960 | tf_op jit(solution)/shard_map/all_gather | solution.py:19
  103.5 0.1 multiply_convert_fusion
  103.7 0.2 convolution_convert_fusion.2
  103.9 1.7 convolution_convert_fusion.3
  105.6 0.3 convolution_convert_fusion.4
  105.8 1.5 convolution_convert_fusion.5
  107.3 0.2 dynamic-update-slice.1
  107.5 5.8 %all-reduce.1 = f32[64]{0:T(128)S(1)} all-reduce(f32[64]{0:T(128)S(1)} %dynamic-update-slice.1), channel_id=3, replica_groups=mesh['grp'=2,'tp'=4,'dp'=4] {'dp'}, use_global_device_ids=true, to_apply=%add.1 | all-reduce | flops 64 | bytes 512
  113.4 0.1 reshape.53
  113.4 0.6 pad_maximum_fusion.2
  114.1 0.1 add_rsqrt_fusion.2
  114.2 28.8 %all-reduce.9.cloned.1.call-done = bf16[16,2048]{1,0:T(8,128)(2,1)} async-done(((bf16[16,2048]{1,0:T(8,128)(2,1)}), bf16[16,2048]{1,0:T(8,128)(2,1)}) %all-reduce.9.cloned.1.call-update) | async-done | bytes 65552 | tf_op jit(solution)/shard_map/psum | solution.py:33
  143.0 0.8 dynamic-slice_convert_fusion
  143.8 0.1 multiply_add_fusion.2
  144.0 2.6 %multiply_add_fusion.1 = (f32[1,4,4,128,128]{4,3,2,1,0:T(8,128)S(1)}, f32[1,4,4,128,128]{4,3,2,1,0:T(8,128)S(1)}) fusion(f32[2,4,4,128,128]{4,3,2,1,0:T(8,128)} %param.19, f32[4,4,128]{2,1,0:T(4,128)S(1)} %mul.268, f32[4,4,128]{2,1,0:T(4,128)S(1)} %mul.265, f32[4,4,128]{2,1,0:T(4,128)S(1)} %mul.261, f32[4,4,128]{2,1,0:T(4,128)S(1)} %mul.296, ...), kind=kLoop, calls=%fused_computation.28 | loop fusion | flops 1572864 | bytes 4243456 | tf_op jit(solution)/shard_map/add | solution.py:51
  146.6 0.7 fusion.2
  147.3 0.1 multiply_reduce_fusion.2
  147.4 0.1 multiply_bitcast_fusion
  147.5 0.1 fusion.44
  147.6 5.2 %all-gather.5 = bf16[4,4,512]{2,1,0:T(4,128)(2,1)S(1)} all-gather(bf16[1,4,512]{2,1,0:T(4,128)(2,1)S(1)} %fusion.44), channel_id=1, replica_groups=mesh['grp'=2,'tp'=4,'dp'=4] {'dp'}, dimensions={0}, use_global_device_ids=true | all-gather | bytes 20480 | tf_op jit(solution)/shard_map/all_gather | solution.py:66
  152.8 1.5 convolution_convert_fusion
  154.3 19.0 %all-reduce.3 = bf16[16,1024]{1,0:T(8,128)(2,1)S(1)} all-reduce(bf16[16,1024]{1,0:T(8,128)(2,1)S(1)} %convolution_convert_fusion), channel_id=5, replica_groups=mesh['grp'=2,'tp'=4,'dp'=4] {'tp'}, use_global_device_ids=true, to_apply=%region_9.0.clone | all-reduce | flops 16384 | bytes 65536
  173.3 0.6 add_convert_fusion
  173.9 1.5 pad_maximum_fusion
  (43 shorter events, 0.4 us)
Async XLA Ops:
  7.2 19.1 %copy-start.1 = (bf16[2,1024,512]{2,1,0:T(8,128)(2,1)S(1)}, bf16[2,1024,512]{2,1,0:T(8,128)(2,1)}, u32[]{:S(2)}) copy-start(bf16[2,1024,512]{2,1,0:T(8,128)(2,1)} %param.13) | copy-start | bytes 6291460
  7.2 54.4 %all-reduce.7.cloned.1.call-start = ((), (), s32[]{:S(2)}) async-start(), calls=%async_computation | async-start | bytes 131072 | tf_op jit(solution)/shard_map/psum | solution.py:33
  23.3 5.6 %copy-start.6 = (f32[2,128]{1,0:T(2,128)S(1)}, f32[2,128]{1,0:T(2,128)}, u32[]{:S(2)}) copy-start(f32[2,128]{1,0:T(2,128)} %param.17) | copy-start | bytes 3076
  23.3 5.6 %copy-start.5 = (f32[2,512]{1,0:T(2,128)S(1)}, f32[2,512]{1,0:T(2,128)}, u32[]{:S(2)}) copy-start(f32[2,512]{1,0:T(2,128)} %param.16) | copy-start | bytes 12292
  23.3 5.7 %copy-start.8 = (u32[32]{0:T(128)S(1)}, u32[32]{0:T(128)}, u32[]{:S(2)}) copy-start(u32[32]{0:T(128)} %constant.30) | copy-start | bytes 388
  23.3 13.0 %copy-start.7 = (u32[32]{0:T(128)S(1)}, u32[32]{0:T(128)}, u32[]{:S(2)}) copy-start(u32[32]{0:T(128)} %constant.42) | copy-start | bytes 388
  26.5 63.8 %copy-start.4 = (bf16[4,1024]{1,0:T(4,128)(2,1)S(1)}, bf16[4,1024]{1,0:T(4,128)(2,1)}, u32[]{:S(2)}) copy-start(bf16[4,1024]{1,0:T(4,128)(2,1)} %param.10) | copy-start | bytes 24580
  26.5 77.1 %copy-start = (bf16[2,1024,512]{2,1,0:T(8,128)(2,1)S(1)}, bf16[2,1024,512]{2,1,0:T(8,128)(2,1)}, u32[]{:S(2)}) copy-start(bf16[2,1024,512]{2,1,0:T(8,128)(2,1)} %param.15) | copy-start | bytes 6291460
  28.8 114.2 %all-reduce.9.cloned.1.call-start = ((), (), s32[]{:S(2)}) async-start(), calls=%async_computation.1 | async-start | bytes 131072 | tf_op jit(solution)/shard_map/psum | solution.py:33
  103.5 2.1 %copy-start.2 = (bf16[2,1024,512]{2,1,0:T(8,128)(2,1)S(1)}, bf16[2,1024,512]{2,1,0:T(8,128)(2,1)}, u32[]{:S(2)}) copy-start(bf16[2,1024,512]{2,1,0:T(8,128)(2,1)} %param.13) | copy-start | bytes 6291460
  144.0 2.6 %copy-start.3 = (f32[2,4,4,128,128]{4,3,2,1,0:T(8,128)S(1)}, f32[2,4,4,128,128]{4,3,2,1,0:T(8,128)}, u32[]{:S(2)}) copy-start(f32[2,4,4,128,128]{4,3,2,1,0:T(8,128)} %param.19) | copy-start | bytes 6291460
Sparse Core Ops, SparseCore 0:
  29.0 32.5 all-reduce.6
  114.2 28.7 all-reduce.8
